TPU v7x, 32 devices: a whole 2x2x4 slice. The times are simulated.
32 devices in a mesh: ep: 4 (over y, x), tp: 8 (over z, core).
Axes of the slice: x: 2, y: 2, z: 4, core: 2. Of those that a mesh axis runs over, the one named last changes fastest.
Arguments:
- features: bfloat16 [64, 1024], P('ep', 'tp'), may hold values from -6 to 6
- key_table: bfloat16 [65536, 1024], P('ep', 'tp'), may hold values from -0.1875 to 0.1875
- value_table: bfloat16 [65536, 1024], P('ep', 'tp'), may hold values from -6 to 6
- chosen: int32 [64, 4, 16], P('ep'), may hold values from 0 to 65535
- scores: float32 [64, 4, 16], P('ep'), may hold values from -8 to 8
Outputs:
- mixed: bfloat16 [64, 1024], P('ep', 'tp')
Inputs may be any that keep to these rules, and one draw needn't show every extreme that they name: Every chosen row is a row of the tables, 0 to 65535; rows may repeat, and a few rows are far more popular than the rest.
All inputs are finite; a program needn't handle non-finite values.
Results may differ from a plain program's by a relative error of at most 0.0065.
Values may be sent and summed in bfloat16 or wider, within the bound.
A program may use at most 64 MiB of HBM per device.

v0:
```python
import jax
import jax.numpy as jnp
from jax import lax
from jax.sharding import PartitionSpec as P


def in_blocks(func, arrays):
    total = arrays[0].shape[0]
    width = 32 if total % 32 == 0 else total
    count = total // width
    if count == 1:
        return func(arrays)
    shaped = tuple((item.reshape((count, width) + item.shape[1:]) for item in arrays))
    result = lax.map(func, shaped)
    return result.reshape((total,) + result.shape[2:])


def shards(features, key_table, value_table, chosen, scores):
    table_rows = key_table.shape[0]
    head_count = chosen.shape[1]
    top_count = chosen.shape[2]
    first_row = lax.axis_index("ep") * table_rows
    gate_weights = jax.nn.softmax(scores, axis=-1)
    chosen_all = lax.all_gather(chosen, "ep", axis=0, tiled=True)
    gates_all = lax.all_gather(gate_weights, "ep", axis=0, tiled=True)
    shifted = chosen_all - first_row
    owned_mask = (shifted >= 0) & (shifted < table_rows)
    local_rows = jnp.clip(shifted, 0, table_rows - 1).reshape(shifted.shape[0], -1)

    def dots_block(pair):
        token_block, picked = pair
        dense = lax.dot_general(
            token_block, key_table, (((1,), (1,)), ((), ())), preferred_element_type=jnp.float32
        )
        return jnp.take_along_axis(dense, picked, axis=1)

    def partial_dots(token_block):
        row_count = token_block.shape[0]
        picked = lax.slice_in_dim(local_rows, 0, row_count, axis=0)
        keep_mask = lax.slice_in_dim(owned_mask, 0, row_count, axis=0)
        products = in_blocks(dots_block, (token_block, picked))
        return jnp.where(keep_mask.reshape(row_count, -1), products, 0.0)

    partial_value = partial_dots(lax.all_gather(features, "ep", axis=0, tiled=True))
    partial_value = partial_value.reshape(-1, head_count, top_count)
    products = lax.psum(partial_value, "tp")
    row_weights = (gates_all * jax.nn.gelu(products, approximate=False)).astype(jnp.bfloat16)
    row_weights = jnp.where(owned_mask, row_weights, jnp.zeros_like(row_weights))
    flat_weights = row_weights.reshape(row_weights.shape[0], -1)

    def value_block(pair):
        block_weights, picked = pair
        width = picked.shape[0]
        token_ids = lax.broadcasted_iota(jnp.int32, picked.shape, 0)
        dense = (
            jnp.zeros((width, table_rows), jnp.float32)
            .at[token_ids, picked]
            .add(block_weights.astype(jnp.float32))
        )
        upper = dense.astype(jnp.bfloat16)
        lower = (dense - upper.astype(jnp.float32)).astype(jnp.bfloat16)
        summed = jnp.dot(upper, value_table, preferred_element_type=jnp.float32)
        return summed + jnp.dot(lower, value_table, preferred_element_type=jnp.float32)

    def owner_term(row_count):
        picked = lax.slice_in_dim(local_rows, 0, row_count, axis=0)
        block_weights = lax.slice_in_dim(flat_weights, 0, row_count, axis=0)
        return in_blocks(value_block, (block_weights, picked))

    summed = lax.psum_scatter(
        owner_term(lax.axis_size("ep") * features.shape[0]), "ep", scatter_dimension=0, tiled=True
    )
    return summed.astype(jnp.bfloat16)


def solution(mesh):
    return jax.shard_map(
        shards,
        mesh=mesh,
        in_specs=(
            P("ep", "tp"),
            P("ep", "tp"),
            P("ep", "tp"),
            P("ep", None, None),
            P("ep", None, None),
        ),
        out_specs=P("ep", "tp"),
        check_vma=False,
    )
```

profile of v0, /device:TPU:0, one launch (start us, length us, event | category | flops | bytes accessed | tf_op | source)
XLA Modules:
  0.0 150.6 jit_solution(2925781054300284029)
XLA Ops:
  0.0 10.1 %all_gather.9 = s32[64,4,16]{2,1,0:T(4,128)S(1)} all-gather(s32[16,4,16]{2,1,0:T(4,128)} %param.12), channel_id=1, replica_groups=mesh['ep'=4,'tp'=8] {'ep'}, dimensions={0}, use_global_device_ids=true | all-gather | bytes 20480 | tf_op jit(solution)/shard_map/all_gather | solution.py:24
  10.1 0.1 copy.12
  10.2 0.1 reshape_reshape.7
  10.3 0.1 copy.16
  10.4 8.0 %all_gather.11 = bf16[64,128]{1,0:T(8,128)(2,1)S(1)} all-gather(bf16[16,128]{1,0:T(8,128)(2,1)} %param.9), channel_id=1, replica_groups=mesh['ep'=4,'tp'=8] {'ep'}, dimensions={0}, use_global_device_ids=true | all-gather | bytes 20480 | tf_op jit(solution)/shard_map/all_gather | solution.py:44
  18.4 0.0 copy-start.3
  18.4 0.0 copy-start.1
  18.4 0.0 copy-start.2
  18.4 41.2 %while.20 = (s32[]{:T(128)}, f32[2,32,64]{2,1,0:T(8,128)S(1)}, s32[2,32,64]{2,1,0:T(8,128)S(1)}, bf16[2,32,128]{2,1,0:T(8,128)(2,1)S(1)}, bf16[16384,128]{1,0:T(8,128)(2,1)}, /*index=5*/s32[]{:T(128)}) while((s32[]{:T(128)}, f32[2,32,64]{2,1,0:T(8,128)S(1)}, s32[2,32,64]{2,1,0:T(8,128)S(1)}, bf16[2,32,128]{2,1,0:T(8,128)(2,1)S(1)}, ...), condition=%wide.region_3.4_spmd, body=%wide.region_2.3_spmd.sunk | while | flops 134248448 | bytes 6430801 | solution.py:14
  18.4 3.7 %fusion.47 = f32[32,16384]{1,0:T(8,128)S(1)} fusion(bf16[16384,128]{1,0:T(8,128)(2,1)} %get-tuple-element.181, bf16[2,32,128]{2,1,0:T(8,128)(2,1)S(1)} %get-tuple-element.180, s32[]{:T(128)} %get-tuple-element.171), kind=kOutput, calls=%fused_computation.8.clone.1 | convolution fusion | flops 134217728 | bytes 6299652 | tf_op jit(solution)/shard_map/while/body/eval_jaxpr/dot_general | solution.py:32
  22.2 0.1 reshape.128
  22.2 16.6 %gather_fusion = f32[2048]{0:T(1024)S(1)} fusion(f32[32,16384]{1,0:T(8,128)S(1)} %fusion.47, s32[2048]{0:T(1024)S(1)} %reshape.128), kind=kCustom, calls=%fused_computation.clone.1 | custom fusion | bytes 32768 | tf_op jit(solution)/shard_map/while/body/eval_jaxpr/jit(take_along_axis)/gather | solution.py:35
  38.9 0.1 gather.11
  39.0 3.7 %fusion.47 = f32[32,16384]{1,0:T(8,128)S(1)} fusion(bf16[16384,128]{1,0:T(8,128)(2,1)} %get-tuple-element.181, bf16[2,32,128]{2,1,0:T(8,128)(2,1)S(1)} %get-tuple-element.180, s32[]{:T(128)} %get-tuple-element.171), kind=kOutput, calls=%fused_computation.8.clone.1 | convolution fusion | flops 134217728 | bytes 6299652 | tf_op jit(solution)/shard_map/while/body/eval_jaxpr/dot_general | solution.py:32
  42.7 0.1 reshape.128
  42.8 16.6 %gather_fusion = f32[2048]{0:T(1024)S(1)} fusion(f32[32,16384]{1,0:T(8,128)S(1)} %fusion.47, s32[2048]{0:T(1024)S(1)} %reshape.128), kind=kCustom, calls=%fused_computation.clone.1 | custom fusion | bytes 32768 | tf_op jit(solution)/shard_map/while/body/eval_jaxpr/jit(take_along_axis)/gather | solution.py:35
  59.5 0.1 gather.11
  59.6 0.1 copy.14
  59.6 0.1 reshape.94
  59.8 26.0 %psum.7 = f32[64,4,16]{0,2,1:T(8,128)S(1)} all-reduce(f32[64,4,16]{0,2,1:T(8,128)S(1)} %get-tuple-element.101), channel_id=1, replica_groups=mesh['ep'=4,'tp'=8] {'tp'}, use_global_device_ids=true, to_apply=%region_4.5 | all-reduce | flops 4096 | bytes 32768 | tf_op jit(solution)/shard_map/psum | solution.py:46
  85.8 0.0 copy-done.3
  85.8 0.2 fusion.17
  86.0 7.7 %all_gather.10 = f32[64,4,16]{2,1,0:T(4,128)S(1)} all-gather(f32[16,4,16]{2,1,0:T(4,128)S(1)} %fusion.17), channel_id=1, replica_groups=mesh['ep'=4,'tp'=8] {'ep'}, dimensions={0}, use_global_device_ids=true | all-gather | bytes 20480 | tf_op jit(solution)/shard_map/all_gather | solution.py:25
  93.6 0.1 copy.15
  93.7 0.1 fusion.30
  93.8 0.1 reshape_reshape.8
  93.9 0.1 copy.17
  94.0 0.0 copy-done.1
  94.0 0.0 copy-done.2
  94.0 0.0 copy-start.4
  94.0 39.5 %while.21 = (s32[]{:T(128)}, f32[2,32,128]{2,1,0:T(8,128)S(1)}, s32[2,32,64]{2,1,0:T(8,128)S(1)}, bf16[2,32,64]{2,1,0:T(8,128)(2,1)S(1)}, bf16[16384,128]{1,0:T(...) while((s32[]{:T(128)}, f32[2,32,128]{2,1,0:T(8,128)S(1)}, ...), condition=%wide.region_7.8_spmd, body=%wide.region_5.7_spmd.sunk | while | flops 271101952 | bytes 35831960 | solution.py:14
  94.1 0.1 multiply_reduce_fusion.2
  94.1 0.1 and_reduce_fusion.2
  94.2 0.1 reshape.131
  94.3 0.1 reshape.132
  94.4 13.3 %scatter_custom_fusion.5 = f32[524288]{0:T(1024)} fusion(s32[2048]{0:T(1024)S(1)} %reshape.131, f32[2048]{0:T(1024)S(1)} %reshape.132, f32[]{:T(128)} %constant.53.clone.1..sunk), kind=kCustom, calls=%fused_computation.16.clone.1 | custom fusion | flops 2048 | bytes 2097156 | tf_op jit(solution)/shard_map/while
  107.7 1.7 %reshape.133 = f32[32,16384]{1,0:T(8,128)S(1)} reshape(f32[524288]{0:T(1024)} %scatter_custom_fusion.5) | data formatting | bytes 4194304 | tf_op jit(solution)/shard_map/while/body/eval_jaxpr/scatter-add | solution.py:58
  109.5 0.0 copy-start
  109.5 3.1 %fusion.53 = f32[32,128]{1,0:T(8,128)S(1)} fusion(bf16[16384,128]{1,0:T(8,128)(2,1)} %get-tuple-element.205, f32[32,16384]{1,0:T(8,128)S(1)} %reshape.133), kind=kOutput, calls=%fused_computation.19.clone.1 | convolution fusion | flops 134742016 | bytes 6307840 | tf_op jit(solution)/shard_map/while/body/eval_jaxpr/dot_general | solution.py:62
  112.6 0.3 copy-done
  112.9 0.8 fusion.54
  113.8 0.1 multiply_reduce_fusion.2
  113.8 0.1 and_reduce_fusion.2
  113.9 0.1 reshape.131
  114.0 0.1 reshape.132
  114.1 13.5 %scatter_custom_fusion.5 = f32[524288]{0:T(1024)} fusion(s32[2048]{0:T(1024)S(1)} %reshape.131, f32[2048]{0:T(1024)S(1)} %reshape.132, f32[]{:T(128)} %constant.53.clone.1..sunk), kind=kCustom, calls=%fused_computation.16.clone.1 | custom fusion | flops 2048 | bytes 2097156 | tf_op jit(solution)/shard_map/while
  127.6 1.7 %reshape.133 = f32[32,16384]{1,0:T(8,128)S(1)} reshape(f32[524288]{0:T(1024)} %scatter_custom_fusion.5) | data formatting | bytes 4194304 | tf_op jit(solution)/shard_map/while/body/eval_jaxpr/scatter-add | solution.py:58
  129.3 0.0 copy-start
  129.3 3.1 %fusion.53 = f32[32,128]{1,0:T(8,128)S(1)} fusion(bf16[16384,128]{1,0:T(8,128)(2,1)} %get-tuple-element.205, f32[32,16384]{1,0:T(8,128)S(1)} %reshape.133), kind=kOutput, calls=%fused_computation.19.clone.1 | convolution fusion | flops 134742016 | bytes 6307840 | tf_op jit(solution)/shard_map/while/body/eval_jaxpr/dot_general | solution.py:62
  132.4 0.3 copy-done
  132.8 0.8 fusion.54
  133.6 15.1 %all-reduce = bf16[64,128]{1,0:T(8,128)(2,1)S(1)} all-reduce(f32[64,128]{1,0:T(8,128)S(1)} %bitcast.41), channel_id=2, replica_groups=mesh['ep'=4,'tp'=8] {'ep'}, use_global_device_ids=true, to_apply=%region_8.9.clone | all-reduce | flops 8192 | bytes 49152
  148.7 0.0 copy-done.4
  148.7 0.6 dynamic-slice
  150.0 0.6 dynamic-slice_convert_fusion.1
  (16 shorter events, 0.2 us)
Async XLA Ops:
  18.4 67.4 %copy-start.3 = (f32[16,4,16]{2,1,0:T(4,128)S(1)}, f32[16,4,16]{2,1,0:T(4,128)}, u32[]{:S(2)}) copy-start(f32[16,4,16]{2,1,0:T(4,128)} %param.13) | copy-start | bytes 12292
  18.4 75.6 %copy-start.1 = (s32[2]{0:T(128)S(1)}, s32[2]{0:T(128)}, u32[]{:S(2)}) copy-start(s32[2]{0:T(128)} %constant.199) | copy-start | bytes 28
  18.4 75.6 %copy-start.2 = (s32[2]{0:T(128)S(1)}, s32[2]{0:T(128)}, u32[]{:S(2)}) copy-start(s32[2]{0:T(128)} %constant.200) | copy-start | bytes 28
  94.0 54.7 %copy-start.4 = (u32[32]{0:T(128)S(1)}, u32[32]{0:T(128)}, u32[]{:S(2)}) copy-start(u32[32]{0:T(128)} %constant.148) | copy-start | bytes 388
  109.5 3.5 %copy-start = (bf16[16384,128]{1,0:T(8,128)(2,1)S(1)}, bf16[16384,128]{1,0:T(8,128)(2,1)}, u32[]{:S(2)}) copy-start(bf16[16384,128]{1,0:T(8,128)(2,1)} %get-tuple-element.205) | copy-start | bytes 12582916 | tf_op jit(solution)/shard_map/while
  129.3 3.5 %copy-start = (bf16[16384,128]{1,0:T(8,128)(2,1)S(1)}, bf16[16384,128]{1,0:T(8,128)(2,1)}, u32[]{:S(2)}) copy-start(bf16[16384,128]{1,0:T(8,128)(2,1)} %get-tuple-element.205) | copy-start | bytes 12582916 | tf_op jit(solution)/shard_map/while
where the time goes:
time: 151 us
  blocking collectives  66.9 us (44%)
  local copies, waits for them, and re-layouts  40 us (26%)
  other arithmetic  27.6 us (18%)
  matrix products  15.2 us (10%)
    gather x6, local copies, waits for them, and re-layouts, dots_block(): return jnp.take_along_axis(dense, picked, axis=1)  33.6 us
    while x8, other arithmetic  27.1 us
    psum x1, blocking collectives, shards(): products = lax.psum(partial_value, 'tp')  26 us
    unnamed x1, blocking collectives  15.1 us
    all_gather x1, blocking collectives, shards(): chosen_all = lax.all_gather(chosen, 'ep', axis=0, tiled=True)  10.1 us
    all_gather x1, blocking collectives, shards(): lax.all_gather(features, 'ep', axis=0, tiled=True)  7.96 us
    all_gather x1, blocking collectives, shards(): gates_all = lax.all_gather(gate_weights, 'ep', axis=0, tiled=True)  7.69 us
    dot_general x2, matrix products, dots_block(): lax.dot_general(token_block, key_table, (((1,), (1,)), ((), ())), preferr...  7.45 us

commit v1 on v0

--- a/solution.py
+++ b/solution.py
@@ -2,6 +2,11 @@
 import jax.numpy as jnp
 from jax import lax
 from jax.sharding import PartitionSpec as P
+
+
+def detail_stacks_all_all(raw):
+    z = lax.all_gather(raw, axis_name="tp")
+    return jnp.sum(z, axis=0)
 
 
 def in_blocks(func, arrays):
@@ -43,7 +48,7 @@
 
     partial_value = partial_dots(lax.all_gather(features, "ep", axis=0, tiled=True))
     partial_value = partial_value.reshape(-1, head_count, top_count)
-    products = lax.psum(partial_value, "tp")
+    products = detail_stacks_all_all(partial_value)
     row_weights = (gates_all * jax.nn.gelu(products, approximate=False)).astype(jnp.bfloat16)
     row_weights = jnp.where(owned_mask, row_weights, jnp.zeros_like(row_weights))
     flat_weights = row_weights.reshape(row_weights.shape[0], -1)

time: 151 us -> 143 us (0.947)
  blocking collectives: 66.9 us -> 58.4 us
    psum x1 -> x0, blocking collectives: 26 us -> none  [shards(): products = lax.psum(partial_value, 'tp')]
    all_gather x0 -> x1, blocking collectives: none -> 17.4 us  [detail_stacks_all_all(): z = lax.all_gather(raw, axis_name='tp')]
where the time goes in v1:
time: 143 us; the launch traced here: 142 us
  blocking collectives  58.4 us (41%)
  local copies, waits for them, and re-layouts  40.2 us (28%)
  other arithmetic  27.8 us (19%)
  matrix products  15.2 us (11%)
    gather x6, local copies, waits for them, and re-layouts, dots_block(): return jnp.take_along_axis(dense, picked, axis=1)  33.6 us
    while x8, other arithmetic  27.1 us
    all_gather x1, blocking collectives, detail_stacks_all_all(): z = lax.all_gather(raw, axis_name='tp')  17.4 us
    unnamed x1, blocking collectives  15.1 us
    all_gather x1, blocking collectives, shards(): chosen_all = lax.all_gather(chosen, 'ep', axis=0, tiled=True)  10.1 us
    all_gather x1, blocking collectives, shards(): lax.all_gather(features, 'ep', axis=0, tiled=True)  7.96 us
    all_gather x1, blocking collectives, shards(): gates_all = lax.all_gather(gate_weights, 'ep', axis=0, tiled=True)  7.69 us
    dot_general x2, matrix products, dots_block(): lax.dot_general(token_block, key_table, (((1,), (1,)), ((), ())), preferr...  7.43 us

profile of v1, /device:TPU:0, one launch (start us, length us, event | category | flops | bytes accessed | tf_op | source)
XLA Modules:
  0.0 142.5 jit_solution(919325881156060888)
XLA Ops:
  0.0 10.1 %all_gather.12 = s32[64,4,16]{2,1,0:T(4,128)S(1)} all-gather(s32[16,4,16]{2,1,0:T(4,128)} %param.12), channel_id=1, replica_groups=mesh['ep'=4,'tp'=8] {'ep'}, dimensions={0}, use_global_device_ids=true | all-gather | bytes 20480 | tf_op jit(solution)/shard_map/all_gather | solution.py:29
  10.1 0.1 copy.26
  10.2 0.1 reshape_reshape.7
  10.3 0.1 copy.33
  10.4 8.0 %all_gather.14 = bf16[64,128]{1,0:T(8,128)(2,1)S(1)} all-gather(bf16[16,128]{1,0:T(8,128)(2,1)} %param.9), channel_id=1, replica_groups=mesh['ep'=4,'tp'=8] {'ep'}, dimensions={0}, use_global_device_ids=true | all-gather | bytes 20480 | tf_op jit(solution)/shard_map/all_gather | solution.py:49
  18.4 41.1 %while.20 = (s32[]{:T(128)}, f32[2,32,64]{2,1,0:T(8,128)S(1)}, s32[2,32,64]{2,1,0:T(8,128)S(1)}, bf16[2,32,128]{2,1,0:T(8,128)(2,1)S(1)}, bf16[16384,128]{1,0:T(8,128)(2,1)}, /*index=5*/s32[]{:T(128)}) while((s32[]{:T(128)}, f32[2,32,64]{2,1,0:T(8,128)S(1)}, s32[2,32,64]{2,1,0:T(8,128)S(1)}, bf16[2,32,128]{2,1,0:T(8,128)(2,1)S(1)}, ...), condition=%wide.region_3.4_spmd, body=%wide.region_2.3_spmd.sunk | while | flops 134248448 | bytes 6430801 | solution.py:19
  18.4 3.7 %fusion.47 = f32[32,16384]{1,0:T(8,128)S(1)} fusion(bf16[16384,128]{1,0:T(8,128)(2,1)} %get-tuple-element.201, bf16[2,32,128]{2,1,0:T(8,128)(2,1)S(1)} %get-tuple-element.200, s32[]{:T(128)} %get-tuple-element.191), kind=kOutput, calls=%fused_computation.8.clone.1 | convolution fusion | flops 134217728 | bytes 6299652 | tf_op jit(solution)/shard_map/while/body/eval_jaxpr/dot_general | solution.py:37
  22.1 0.1 reshape.131
  22.2 16.6 %gather_fusion = f32[2048]{0:T(1024)S(1)} fusion(f32[32,16384]{1,0:T(8,128)S(1)} %fusion.47, s32[2048]{0:T(1024)S(1)} %reshape.131), kind=kCustom, calls=%fused_computation.clone.1 | custom fusion | bytes 32768 | tf_op jit(solution)/shard_map/while/body/eval_jaxpr/jit(take_along_axis)/gather | solution.py:40
  38.8 0.1 gather.11
  38.9 3.7 %fusion.47 = f32[32,16384]{1,0:T(8,128)S(1)} fusion(bf16[16384,128]{1,0:T(8,128)(2,1)} %get-tuple-element.201, bf16[2,32,128]{2,1,0:T(8,128)(2,1)S(1)} %get-tuple-element.200, s32[]{:T(128)} %get-tuple-element.191), kind=kOutput, calls=%fused_computation.8.clone.1 | convolution fusion | flops 134217728 | bytes 6299652 | tf_op jit(solution)/shard_map/while/body/eval_jaxpr/dot_general | solution.py:37
  42.7 0.1 reshape.131
  42.8 16.6 %gather_fusion = f32[2048]{0:T(1024)S(1)} fusion(f32[32,16384]{1,0:T(8,128)S(1)} %fusion.47, s32[2048]{0:T(1024)S(1)} %reshape.131), kind=kCustom, calls=%fused_computation.clone.1 | custom fusion | bytes 32768 | tf_op jit(solution)/shard_map/while/body/eval_jaxpr/jit(take_along_axis)/gather | solution.py:40
  59.4 0.1 gather.11
  59.5 0.0 copy-start.3
  59.5 0.0 copy-start.1
  59.5 0.0 copy-start.2
  59.5 0.1 copy.28
  59.6 0.1 reshape.96
  59.8 0.1 copy.29
  59.9 17.4 %all-gather = f32[512,4,16]{2,1,0:T(4,128)S(1)} all-gather(f32[64,4,16]{2,1,0:T(4,128)S(1)} %copy.29), channel_id=2, replica_groups=mesh['ep'=4,'tp'=8] {'tp'}, dimensions={0}, use_global_device_ids=true | all-gather | bytes 147456 | tf_op jit(solution)/shard_map/all_gather | solution.py:8
  77.3 0.3 reduce_sum.19
  77.6 0.1 copy.30
  77.7 0.0 copy-done.3
  77.7 0.2 fusion.17
  77.9 7.7 %all_gather.13 = f32[64,4,16]{2,1,0:T(4,128)S(1)} all-gather(f32[16,4,16]{2,1,0:T(4,128)S(1)} %fusion.17), channel_id=1, replica_groups=mesh['ep'=4,'tp'=8] {'ep'}, dimensions={0}, use_global_device_ids=true | all-gather | bytes 20480 | tf_op jit(solution)/shard_map/all_gather | solution.py:30
  85.5 0.1 copy.32
  85.6 0.1 fusion.30
  85.7 0.1 reshape_reshape.8
  85.8 0.1 copy.34
  85.9 0.0 copy-done.1
  85.9 0.0 copy-done.2
  85.9 0.0 copy-start.4
  85.9 39.5 %while.21 = (s32[]{:T(128)}, f32[2,32,128]{2,1,0:T(8,128)S(1)}, s32[2,32,64]{2,1,0:T(8,128)S(1)}, bf16[2,32,64]{2,1,0:T(8,128)(2,1)S(1)}, bf16[16384,128]{1,0:T(...) while((s32[]{:T(128)}, f32[2,32,128]{2,1,0:T(8,128)S(1)}, ...), condition=%wide.region_7.8_spmd, body=%wide.region_5.7_spmd.sunk | while | flops 271101952 | bytes 35831960 | solution.py:19
  86.0 0.1 multiply_reduce_fusion.2
  86.1 0.1 and_reduce_fusion.2
  86.1 0.1 reshape.134
  86.2 0.1 reshape.135
  86.3 13.3 %scatter_custom_fusion.5 = f32[524288]{0:T(1024)} fusion(s32[2048]{0:T(1024)S(1)} %reshape.134, f32[2048]{0:T(1024)S(1)} %reshape.135, f32[]{:T(128)} %constant.26.clone.1..sunk), kind=kCustom, calls=%fused_computation.16.clone.1 | custom fusion | flops 2048 | bytes 2097156 | tf_op jit(solution)/shard_map/while
  99.6 1.7 %reshape.136 = f32[32,16384]{1,0:T(8,128)S(1)} reshape(f32[524288]{0:T(1024)} %scatter_custom_fusion.5) | data formatting | bytes 4194304 | tf_op jit(solution)/shard_map/while/body/eval_jaxpr/scatter-add | solution.py:63
  101.4 0.0 copy-start
  101.4 3.1 %fusion.53 = f32[32,128]{1,0:T(8,128)S(1)} fusion(bf16[16384,128]{1,0:T(8,128)(2,1)} %get-tuple-element.225, f32[32,16384]{1,0:T(8,128)S(1)} %reshape.136), kind=kOutput, calls=%fused_computation.19.clone.1 | convolution fusion | flops 134742016 | bytes 6307840 | tf_op jit(solution)/shard_map/while/body/eval_jaxpr/dot_general | solution.py:67
  104.5 0.3 copy-done
  104.8 0.8 fusion.54
  105.7 0.1 multiply_reduce_fusion.2
  105.7 0.1 and_reduce_fusion.2
  105.8 0.1 reshape.134
  105.9 0.1 reshape.135
  106.0 13.5 %scatter_custom_fusion.5 = f32[524288]{0:T(1024)} fusion(s32[2048]{0:T(1024)S(1)} %reshape.134, f32[2048]{0:T(1024)S(1)} %reshape.135, f32[]{:T(128)} %constant.26.clone.1..sunk), kind=kCustom, calls=%fused_computation.16.clone.1 | custom fusion | flops 2048 | bytes 2097156 | tf_op jit(solution)/shard_map/while
  119.5 1.7 %reshape.136 = f32[32,16384]{1,0:T(8,128)S(1)} reshape(f32[524288]{0:T(1024)} %scatter_custom_fusion.5) | data formatting | bytes 4194304 | tf_op jit(solution)/shard_map/while/body/eval_jaxpr/scatter-add | solution.py:63
  121.2 0.0 copy-start
  121.2 3.1 %fusion.53 = f32[32,128]{1,0:T(8,128)S(1)} fusion(bf16[16384,128]{1,0:T(8,128)(2,1)} %get-tuple-element.225, f32[32,16384]{1,0:T(8,128)S(1)} %reshape.136), kind=kOutput, calls=%fused_computation.19.clone.1 | convolution fusion | flops 134742016 | bytes 6307840 | tf_op jit(solution)/shard_map/while/body/eval_jaxpr/dot_general | solution.py:67
  124.3 0.3 copy-done
  124.7 0.8 fusion.54
  125.5 15.1 %all-reduce = bf16[64,128]{1,0:T(8,128)(2,1)S(1)} all-reduce(f32[64,128]{1,0:T(8,128)S(1)} %bitcast.43), channel_id=3, replica_groups=mesh['ep'=4,'tp'=8] {'ep'}, use_global_device_ids=true, to_apply=%region_8.9.clone | all-reduce | flops 8192 | bytes 49152
  140.6 0.0 copy-done.4
  140.6 0.6 dynamic-slice
  141.9 0.6 dynamic-slice_convert_fusion.1
  (16 shorter events, 0.1 us)
Async XLA Ops:
  59.5 18.1 %copy-start.3 = (f32[16,4,16]{2,1,0:T(4,128)S(1)}, f32[16,4,16]{2,1,0:T(4,128)}, u32[]{:S(2)}) copy-start(f32[16,4,16]{2,1,0:T(4,128)} %param.13) | copy-start | bytes 12292
  59.5 26.4 %copy-start.1 = (s32[2]{0:T(128)S(1)}, s32[2]{0:T(128)}, u32[]{:S(2)}) copy-start(s32[2]{0:T(128)} %constant.199) | copy-start | bytes 28
  59.5 26.4 %copy-start.2 = (s32[2]{0:T(128)S(1)}, s32[2]{0:T(128)}, u32[]{:S(2)}) copy-start(s32[2]{0:T(128)} %constant.200) | copy-start | bytes 28
  85.9 54.7 %copy-start.4 = (u32[32]{0:T(128)S(1)}, u32[32]{0:T(128)}, u32[]{:S(2)}) copy-start(u32[32]{0:T(128)} %constant.148) | copy-start | bytes 388
  101.4 3.5 %copy-start = (bf16[16384,128]{1,0:T(8,128)(2,1)S(1)}, bf16[16384,128]{1,0:T(8,128)(2,1)}, u32[]{:S(2)}) copy-start(bf16[16384,128]{1,0:T(8,128)(2,1)} %get-tuple-element.225) | copy-start | bytes 12582916 | tf_op jit(solution)/shard_map/while
  121.2 3.5 %copy-start = (bf16[16384,128]{1,0:T(8,128)(2,1)S(1)}, bf16[16384,128]{1,0:T(8,128)(2,1)}, u32[]{:S(2)}) copy-start(bf16[16384,128]{1,0:T(8,128)(2,1)} %get-tuple-element.225) | copy-start | bytes 12582916 | tf_op jit(solution)/shard_map/while
